TPU v7x, 32 devices: a whole 2x2x4 slice. The times are simulated.
32 devices in a mesh: sp: 8 (over z, y), tp: 4 (over x, core).
Axes of the slice: x: 2, y: 2, z: 4, core: 2. Of those that a mesh axis runs over, the one named last changes fastest.
Arguments:
- queries: bfloat16 [6144, 1024], P('sp', 'tp'), may hold values from -8 to 8
- keys: bfloat16 [6144, 256], P('sp', 'tp'), may hold values from -8 to 8
- values: bfloat16 [6144, 256], P('sp', 'tp'), may hold values from -18 to 18
- query_gain: float32 [64], replicated, may hold values from 0.4 to 5.5
- key_gain: float32 [64], replicated, may hold values from 0.4 to 5.5
- sink_logits: float32 [16], P('tp'), may hold values from 2 to 5
- out_weight: bfloat16 [1024, 2048], P('tp'), may hold values from -0.1875 to 0.1875
- residual: bfloat16 [6144, 2048], P('sp', 'tp'), may hold values from -21 to 21
- norm_gain: float32 [2048], P('tp'), may hold values from 0.1 to 1.9
- gate_weight: bfloat16 [2048, 5632], P('sp', 'tp'), may hold values from -0.125 to 0.125
- up_weight: bfloat16 [2048, 5632], P('sp', 'tp'), may hold values from -0.125 to 0.125
- down_weight: bfloat16 [5632, 2048], P('tp', 'sp'), may hold values from -0.078125 to 0.078125
Outputs:
- layer_out: bfloat16 [6144, 2048], P('sp', 'tp')
All inputs are finite; a program needn't handle non-finite values.
Results may differ from a plain program's by a relative error of at most 0.0095.
The roundings to bfloat16 on the way count: a program that leaves them out, or rounds other values in their place, can miss the bound.
Values may be sent and summed in bfloat16 or wider, within the bound.
No kernel may reach another device: no remote copies, remote signals or barrier semaphores. Data moves between devices by JAX's collectives and lax.ppermute only.
A program may use at most 192 MiB of HBM per device.

v0:
```python
import jax
import jax.numpy as jnp
from jax import lax
from jax.sharding import PartitionSpec as P

D = 2048
WINDOW = 128


def from_behind(block, axis, distance):
    devices = range(lax.axis_size(axis))
    route = [(i - distance, i) for i in devices if i - distance in devices]
    return lax.ppermute(block, axis, route)


def norm_heads(flat, gain, heads):
    row_count = flat.shape[0]
    head_width = gain.shape[0]
    data = flat.astype(jnp.float32).reshape(row_count, heads, head_width)
    scaled = data * lax.rsqrt(jnp.mean(data * data, axis=-1, keepdims=True) + 1e-06) * gain
    return scaled.astype(jnp.bfloat16)


def per_device(
    queries,
    keys,
    values,
    query_gain,
    key_gain,
    sink_logits,
    out_weight,
    residual,
    norm_gain,
    gate_weight,
    up_weight,
    down_weight,
):
    head_width = query_gain.shape[0]
    row_count = queries.shape[0]
    q_heads = queries.shape[1] // head_width
    k_heads = keys.shape[1] // head_width
    group_size = q_heads // k_heads
    window_len = WINDOW
    block_count = row_count // window_len
    gate_full, up_full = (
        lax.all_gather(gate_weight, "sp", axis=0, tiled=True),
        lax.all_gather(up_weight, "sp", axis=0, tiled=True),
    )
    down_full = lax.all_gather(down_weight, "sp", axis=1, tiled=True)
    query_norm = norm_heads(queries, query_gain, q_heads)
    key_norm = norm_heads(keys, key_gain, k_heads).reshape(row_count, k_heads * head_width)
    prev_keys, prev_values = from_behind(
        (key_norm[row_count - window_len :], values[row_count - window_len :]), "sp", 1
    )
    key_all = jnp.concatenate([prev_keys, key_norm], axis=0)
    value_all = jnp.concatenate([prev_values, values], axis=0)
    key_blocks = jnp.concatenate(
        [
            key_all[:row_count].reshape(block_count, window_len, k_heads, head_width),
            key_norm.reshape(block_count, window_len, k_heads, head_width),
        ],
        axis=1,
    )
    value_blocks = jnp.concatenate(
        [
            value_all[:row_count].reshape(block_count, window_len, k_heads, head_width),
            values.reshape(block_count, window_len, k_heads, head_width),
        ],
        axis=1,
    )
    query_blocks = query_norm.reshape(block_count, window_len, k_heads, group_size, head_width)
    scores = jnp.einsum(
        "nqhgd,nkhd->nhgqk", query_blocks, key_blocks, preferred_element_type=jnp.float32
    ) * head_width ** (-0.5)
    query_index = jnp.arange(window_len)[:, None]
    key_index = jnp.arange(2 * window_len)[None, :]
    offset_lag = window_len + query_index - key_index
    inband = (offset_lag >= 0) & (offset_lag < window_len)
    leading = (
        (jnp.arange(block_count)[:, None, None] > 0)
        | (key_index[None] >= window_len)
        | (lax.axis_index("sp") > 0)
    )
    valid = inband[None] & leading
    scores = jnp.where(valid[:, None, None], scores, -1e30)
    sink_rows = sink_logits.reshape(k_heads, group_size)[None, :, :, None]
    row_peak = jnp.maximum(jnp.max(scores, axis=-1), sink_rows)
    exp_terms = jnp.exp(scores - row_peak[..., None])
    denom_sum = jnp.sum(exp_terms, axis=-1) + jnp.exp(sink_rows - row_peak)
    weights = (exp_terms / denom_sum[..., None]).astype(jnp.bfloat16)
    attended = jnp.einsum(
        "nhgqk,nkhd->nqhgd", weights, value_blocks, preferred_element_type=jnp.float32
    ).astype(jnp.bfloat16)
    attended = attended.reshape(row_count, q_heads * head_width)
    projected = jnp.dot(attended, out_weight, preferred_element_type=jnp.float32)
    mixed = lax.psum_scatter(
        projected.astype(jnp.bfloat16), "tp", scatter_dimension=1, tiled=True
    ).astype(jnp.float32)
    middle_wide = (residual.astype(jnp.float32) + mixed).astype(jnp.bfloat16).astype(jnp.float32)
    squares = lax.psum(jnp.sum(middle_wide * middle_wide, axis=1), "tp")
    normed = (middle_wide * lax.rsqrt(squares / D + 1e-06)[:, None] * norm_gain).astype(
        jnp.bfloat16
    )
    normed_all = lax.all_gather(normed, "tp", axis=1, tiled=True)
    gate_acts = jnp.dot(normed_all, gate_full, preferred_element_type=jnp.float32)
    up_acts = jnp.dot(normed_all, up_full, preferred_element_type=jnp.float32)
    hidden = (jax.nn.silu(gate_acts) * up_acts).astype(jnp.bfloat16)
    down_terms = jnp.dot(hidden, down_full, preferred_element_type=jnp.float32)
    summed_back = lax.psum_scatter(
        down_terms.astype(jnp.bfloat16), "tp", scatter_dimension=1, tiled=True
    ).astype(jnp.float32)
    return (middle_wide + 0.5 * summed_back).astype(jnp.bfloat16)


def solution(mesh):
    in_specs = (
        P("sp", "tp"),
        P("sp", "tp"),
        P("sp", "tp"),
        P(),
        P(),
        P("tp"),
        P("tp", None),
        P("sp", "tp"),
        P("tp"),
        P("sp", "tp"),
        P("sp", "tp"),
        P("tp", "sp"),
    )
    out_specs = P("sp", "tp")
    return jax.shard_map(
        per_device, mesh=mesh, in_specs=in_specs, out_specs=out_specs, check_vma=False
    )
```

profile of v0, /device:TPU:0, one launch (start us, length us, event | category | flops | bytes accessed | tf_op | source)
XLA Modules:
  0.0 404.4 jit_solution(5352290155806493148)
XLA Ops:
  7.4 0.0 copy-start
  7.4 0.0 copy-start.4
  7.4 0.0 reduce-scatter.3.cloned.1.call-start
  7.4 1.0 fusion.19
  8.4 1.0 fusion.21
  9.4 4.9 %collective-permute-start.1 = (bf16[128,64]{0,1:T(8,128)(2,1)S(1)}, bf16[128,64]{0,1:T(8,128)(2,1)S(1)}, u32[]{:S(2)}, u32[]{:S(2)}) collective-permute-start(bf16[128,64]{0,1:T(8,128)(2,1)S(1)} %slice.18), channel_id=1, source_target_pairs={{0,4},{4,8},{8,12},{12,16},{16,20},{20,24},{24,28},{1,5},{5,9},{9,... | collective-permute-start | bytes 49160 | tf_op jit(solution)/shard_map/ppermute | solution.py:13
  14.3 0.7 slice.14
  15.0 3.4 collective-permute-start
  18.5 1.2 copy.19
  19.6 0.4 reshape.185
  20.1 0.1 bitcast_reduce_fusion
  20.3 0.8 multiply_convert_fusion.1
  21.1 0.0 copy-start.5
  21.1 0.1 or_or_fusion
  21.2 0.3 broadcast_and_fusion
  21.5 0.1 reshape_reshape.3
  21.6 0.0 copy-done.4
  21.6 0.1 reshape.181
  21.8 0.0 collective-permute-done.1
  21.9 0.1 reshape.183
  22.0 0.6 fusion.1
  22.7 0.0 copy-start.3
  22.7 0.0 copy-done.5
  22.7 0.1 broadcast_maximum_fusion
  22.8 1.6 copy-done.3
  24.3 0.7 fusion
  25.1 0.1 exponential_add_fusion
  25.1 0.0 collective-permute-done
  25.2 0.1 reshape.180
  25.3 2.8 fusion.12
  28.2 0.3 copy.22
  28.4 0.0 copy-done
  28.4 2.7 convolution_convert_fusion
  31.2 0.0 copy-start.1
  31.2 0.0 copy-start.6
  31.2 0.0 reduce-scatter.3.cloned.1.call-update
  31.2 0.0 all-gather.7.cloned.1.call-start
  31.3 0.5 all-gather.7.cloned.1.call-update
  31.8 0.0 all-gather.5.cloned.1.call-start
  31.8 37.5 %reduce-scatter.3.cloned.1.call-done = bf16[768,512]{1,0:T(8,128)(2,1)} async-done(((bf16[768,2048]{1,0:T(8,128)(2,1)}), bf16[768,512]{1,0:T(8,128)(2,1)}) %reduce-scatter.3.cloned.1.call-update) | async-done | bytes 786448 | tf_op jit(solution)/shard_map/reduce_scatter | solution.py:96
  69.3 0.0 copy-done.1
  69.3 1.5 fusion.2
  70.8 5.8 %psum.7 = f32[768]{0:T(1024)S(1)} all-reduce(f32[768]{0:T(1024)S(1)} %fusion.2), channel_id=1, replica_groups=mesh['sp'=8,'tp'=4] {'tp'}, use_global_device_ids=true, to_apply=%region_6.7 | all-reduce | flops 768 | bytes 6144 | tf_op jit(solution)/shard_map/psum | solution.py:100
  76.5 0.0 copy-done.6
  76.5 2.3 fusion.4
  78.9 0.0 all-gather.5.cloned.1.call-update
  78.9 0.0 all-gather.11.cloned.1.call-start
  78.9 0.5 all-gather.11.cloned.1.call-update
  79.5 0.0 all-gather.9.cloned.1.call-start
  79.5 0.7 all-gather.9.cloned.1.call-update
  80.2 0.2 reduce-scatter.5.cloned.1.call-start
  80.4 45.8 %all-gather.7.cloned.1.call-done = bf16[2048,1408]{1,0:T(8,128)(2,1)} async-done(((bf16[256,1408]{1,0:T(8,128)(2,1)}), bf16[2048,1408]{1,0:T(8,128)(2,1)}) %all-gather.7.cloned.1.call-update) | async-done | bytes 5767184 | tf_op jit(solution)/shard_map/all_gather | solution.py:46
  126.3 28.0 %all-gather.5.cloned.1.call-done = bf16[768,2048]{1,0:T(8,128)(2,1)} async-done(((bf16[768,512]{1,0:T(8,128)(2,1)}), bf16[768,2048]{1,0:T(8,128)(2,1)}) %all-gather.5.cloned.1.call-update) | async-done | bytes 3145744 | tf_op jit(solution)/shard_map/all_gather | solution.py:104
  154.3 9.7 %fusion.34 = f32[768,1408]{1,0:T(8,128)} fusion(bf16[768,2048]{1,0:T(8,128)(2,1)} %all-gather.5.cloned.1.call-done, bf16[2048,1408]{1,0:T(8,128)(2,1)} %all-gather.7.cloned.1.call-done), kind=kOutput, calls=%fused_computation.60 | convolution fusion | flops 4429185024 | bytes 13238272 | tf_op jit(solution)/shard_map/dot_general | solution.py:105
  163.9 85.2 %all-gather.11.cloned.1.call-done = bf16[1408,2048]{1,0:T(8,128)(2,1)} async-done(((bf16[1408,256]{1,0:T(8,128)(2,1)}), bf16[1408,2048]{1,0:T(8,128)(2,1)}) %all-gather.11.cloned.1.call-update) | async-done | bytes 5767184 | tf_op jit(solution)/shard_map/all_gather | solution.py:49
  249.1 92.5 %all-gather.9.cloned.1.call-done = bf16[2048,1408]{1,0:T(8,128)(2,1)} async-done(((bf16[256,1408]{1,0:T(8,128)(2,1)}), bf16[2048,1408]{1,0:T(8,128)(2,1)}) %all-gather.9.cloned.1.call-update) | async-done | bytes 5767184 | tf_op jit(solution)/shard_map/all_gather | solution.py:47
  341.6 16.8 %convolution_convert_fusion.1 = bf16[768,2048]{1,0:T(8,128)(2,1)} fusion(bf16[1408,2048]{1,0:T(8,128)(2,1)} %all-gather.11.cloned.1.call-done, f32[768,1408]{1,0:T(8,128)} %fusion.34, bf16[768,2048]{1,0:T(8,128)(2,1)} %all-gather.5.cloned.1.call-done, bf16[2048,1408]{1,0:T(8,128)(2,1)} %all-gather.9.cloned.1.call-done), kind=kOutput, calls=%fused_computation.2 | convolution fusion | flops 8866430976 | bytes 22151168 | tf_op jit(solution)/shard_map/dot_general | solution.py:108
  358.4 0.0 copy-start.2
  358.4 0.0 reduce-scatter.5.cloned.1.call-update
  358.4 36.0 %reduce-scatter.5.cloned.1.call-done = bf16[768,512]{1,0:T(8,128)(2,1)} async-done(((bf16[768,2048]{1,0:T(8,128)(2,1)}), bf16[768,512]{1,0:T(8,128)(2,1)}) %reduce-scatter.5.cloned.1.call-update) | async-done | bytes 786448 | tf_op jit(solution)/shard_map/reduce_scatter | solution.py:109
  394.5 0.0 copy-done.2
  394.5 2.3 fusion.5
  (15 shorter events, 0.2 us)
Async XLA Ops:
  7.4 21.1 %copy-start = (bf16[256,2048]{1,0:T(8,128)(2,1)S(1)}, bf16[256,2048]{1,0:T(8,128)(2,1)}, u32[]{:S(2)}) copy-start(bf16[256,2048]{1,0:T(8,128)(2,1)} %param.18) | copy-start | bytes 3145732
  7.4 14.3 %copy-start.4 = (bf16[768,64]{0,1:T(8,128)(2,1)S(1)}, bf16[768,64]{0,1:T(8,128)(2,1)}, u32[]{:S(2)}) copy-start(bf16[768,64]{0,1:T(8,128)(2,1)} %param.14) | copy-start | bytes 294916
  7.4 61.9 %reduce-scatter.3.cloned.1.call-start = ((), (), s32[]{:S(2)}) async-start(), calls=%async_computation.2 | async-start | bytes 3932160 | tf_op jit(solution)/shard_map/reduce_scatter | solution.py:96
  9.4 12.4 %collective-permute-start.1 = (bf16[128,64]{0,1:T(8,128)(2,1)S(1)}, bf16[128,64]{0,1:T(8,128)(2,1)S(1)}, u32[]{:S(2)}, u32[]{:S(2)}) collective-permute-start(bf16[128,64]{0,1:T(8,128)(2,1)S(1)} %slice.18), channel_id=1, source_target_pairs={{0,4},{4,8},{8,12},{12,16},{16,20},{20,24},{24,28},{1,5},{5,9},{9,... | collective-permute-start | bytes 49160 | tf_op jit(solution)/shard_map/ppermute | solution.py:13
  15.0 10.1 %collective-permute-start = (bf16[128,64]{0,1:T(8,128)(2,1)S(1)}, bf16[128,64]{0,1:T(8,128)(2,1)S(1)}, u32[]{:S(2)}, u32[]{:S(2)}) collective-permute-start(bf16[128,64]{0,1:T(8,128)(2,1)S(1)} %slice.14), channel_id=1, source_target_pairs={{0,4},{4,8},{8,12},{12,16},{16,20},{20,24},{24,28},{1,5},{5,9},{9,... | collective-permute-start | bytes 49160 | tf_op jit(solution)/shard_map/ppermute | solution.py:13
  21.1 1.6 copy-start.5
  22.7 1.6 copy-start.3
  31.2 38.1 %copy-start.1 = (bf16[768,512]{1,0:T(8,128)(2,1)S(1)}, bf16[768,512]{1,0:T(8,128)(2,1)}, u32[]{:S(2)}) copy-start(bf16[768,512]{1,0:T(8,128)(2,1)} %param.19) | copy-start | bytes 2359300
  31.2 45.4 %copy-start.6 = (f32[512]{0:T(512)S(1)}, f32[512]{0:T(512)}, u32[]{:S(2)}) copy-start(f32[512]{0:T(512)} %param.20) | copy-start | bytes 6148
  31.2 95.1 %all-gather.7.cloned.1.call-start = ((), (), s32[]{:S(2)}) async-start(), calls=%async_computation.4 | async-start | bytes 6488064 | tf_op jit(solution)/shard_map/all_gather | solution.py:46
  31.8 122.5 %all-gather.5.cloned.1.call-start = ((), (), s32[]{:S(2)}) async-start(), calls=%async_computation.3 | async-start | bytes 3932160 | tf_op jit(solution)/shard_map/all_gather | solution.py:104
  78.9 170.2 %all-gather.11.cloned.1.call-start = ((), (), s32[]{:S(2)}) async-start(), calls=%async_computation.6 | async-start | bytes 6488064 | tf_op jit(solution)/shard_map/all_gather | solution.py:49
  79.5 262.2 %all-gather.9.cloned.1.call-start = ((), (), s32[]{:S(2)}) async-start(), calls=%async_computation.5 | async-start | bytes 6488064 | tf_op jit(solution)/shard_map/all_gather | solution.py:47
  80.2 314.3 %reduce-scatter.5.cloned.1.call-start = ((), (), s32[]{:S(2)}) async-start(), calls=%async_computation.7 | async-start | bytes 3932160 | tf_op jit(solution)/shard_map/reduce_scatter | solution.py:109
  358.4 36.1 %copy-start.2 = (bf16[768,512]{1,0:T(8,128)(2,1)S(1)}, bf16[768,512]{1,0:T(8,128)(2,1)}, u32[]{:S(2)}) copy-start(bf16[768,512]{1,0:T(8,128)(2,1)} %reduce-scatter.3.cloned.1.call-done) | copy-start | bytes 2359300
Sparse Core Ops, SparseCore 0:
  31.3 37.9 reduce-scatter.2
  358.6 35.8 reduce-scatter.4
Sparse Core Ops, SparseCore 1:
  33.9 92.3 all-gather.6
  127.7 26.5 all-gather.4
  156.2 92.9 all-gather.10
  251.3 90.3 all-gather.8
where the time goes:
time: 405 us; the launch traced here: 404 us
  waiting for transfers between devices  327 us (81%)
  matrix products  32.7 us (8%)
  between operations  15.3 us (4%)
  other arithmetic  10.4 us (3%)
  starting transfers between devices  8.71 us (2%)
  blocking collectives  5.77 us (1%)
  local copies, waits for them, and re-layouts  4.77 us (1%)
    all_gather x1, waiting for transfers between devices, per_device(): lax.all_gather(up_weight, 'sp', axis=0, tiled=True)  92.5 us
    all_gather x1, waiting for transfers between devices, per_device(): down_full = lax.all_gather(down_weight, 'sp', axis=1, tiled=True)  85.2 us
    all_gather x1, waiting for transfers between devices, per_device(): lax.all_gather(gate_weight, 'sp', axis=0, tiled=True)  45.8 us
    reduce_scatter x1, waiting for transfers between devices, per_device(): lax.psum_scatter(projected.astype(jnp.bfloat16), 'tp', scatter_dimension=...  37.5 us
    reduce_scatter x1, waiting for transfers between devices, per_device(): lax.psum_scatter(down_terms.astype(jnp.bfloat16), 'tp', scatter_dimension...  36 us
    all_gather x1, waiting for transfers between devices, per_device(): normed_all = lax.all_gather(normed, 'tp', axis=1, tiled=True)  28 us
    dot_general x1, matrix products, per_device(): down_terms = jnp.dot(hidden, down_full, preferred_element_type=jnp.float32)  16.8 us
    dot_general x1, matrix products, per_device(): jnp.dot(normed_all, gate_full, preferred_element_type=jnp.float32)  9.67 us
  transfers between devices with their start and end apart: 8, of which 6 were waited for; matrix products, arithmetic and copies ran while one was open for 5% of the time, Pallas kernels for 0%

commit v1 on v0

--- a/solution.py
+++ b/solution.py
@@ -5,6 +5,11 @@
 
 D = 2048
 WINDOW = 128
+
+
+def swapped_in(shard, name, along):
+    outgoing = jnp.stack([shard] * lax.axis_size(name))
+    return jnp.concatenate(lax.all_to_all(outgoing, name, 0, 0), axis=along)
 
 
 def from_behind(block, axis, distance):
@@ -44,7 +49,7 @@
     block_count = row_count // window_len
     gate_full, up_full = (
         lax.all_gather(gate_weight, "sp", axis=0, tiled=True),
-        lax.all_gather(up_weight, "sp", axis=0, tiled=True),
+        swapped_in(up_weight, "sp", 0),
     )
     down_full = lax.all_gather(down_weight, "sp", axis=1, tiled=True)
     query_norm = norm_heads(queries, query_gain, q_heads)

time: 405 us -> 392 us (0.968)
  waiting for transfers between devices: 327 us -> 305 us
  starting transfers between devices: 8.71 us -> 14.4 us
    all_gather x1 -> x0, waiting for transfers between devices: 92.5 us -> none  [per_device(): lax.all_gather(up_weight, 'sp', axis=0, tiled=True)]
    all_gather x1, waiting for transfers between devices: 45.8 us -> 83.8 us  [per_device(): lax.all_gather(gate_weight, 'sp', axis=0, tiled=True)]
    all_gather x1, waiting for transfers between devices: 28 us -> 54.1 us  [per_device(): normed_all = lax.all_gather(normed, 'tp', axis=1, tiled=True)]
    all_to_all x0 -> x1, waiting for transfers between devices: none -> 26.1 us  [swapped_in(): return jnp.concatenate(lax.all_to_all(outgoing, name, 0, 0), axis=along)]
    all_gather x1, waiting for transfers between devices: 85.2 us -> 66.4 us  [per_device(): down_full = lax.all_gather(down_weight, 'sp', axis=1, tiled=True)]
    all_to_all x0 -> x1, starting transfers between devices: none -> 5.71 us  [swapped_in(): return jnp.concatenate(lax.all_to_all(outgoing, name, 0, 0), axis=along)]
  transfers between devices with their start and end apart: 8 -> 8, of which waited for: 6 -> 6; matrix products, arithmetic and copies ran while one was open for 5% -> 6% of each run, Pallas kernels for 0% -> 0%
where the time goes in v1:
time: 392 us; the launch traced here: 391 us
  waiting for transfers between devices  305 us (78%)
  matrix products  32.7 us (8%)
  between operations  15.3 us (4%)
  starting transfers between devices  14.4 us (4%)
  other arithmetic  10.4 us (3%)
  local copies, waits for them, and re-layouts  7.69 us (2%)
  blocking collectives  5.77 us (1%)
    all_gather x1, waiting for transfers between devices, per_device(): lax.all_gather(gate_weight, 'sp', axis=0, tiled=True)  83.8 us
    all_gather x1, waiting for transfers between devices, per_device(): down_full = lax.all_gather(down_weight, 'sp', axis=1, tiled=True)  66.4 us
    all_gather x1, waiting for transfers between devices, per_device(): normed_all = lax.all_gather(normed, 'tp', axis=1, tiled=True)  54.1 us
    reduce_scatter x1, waiting for transfers between devices, per_device(): lax.psum_scatter(projected.astype(jnp.bfloat16), 'tp', scatter_dimension=...  37.5 us
    reduce_scatter x1, waiting for transfers between devices, per_device(): lax.psum_scatter(down_terms.astype(jnp.bfloat16), 'tp', scatter_dimension...  36.1 us
    all_to_all x1, waiting for transfers between devices, swapped_in(): return jnp.concatenate(lax.all_to_all(outgoing, name, 0, 0), axis=along)  26.1 us
    dot_general x1, matrix products, per_device(): down_terms = jnp.dot(hidden, down_full, preferred_element_type=jnp.float32)  16.9 us
    dot_general x1, matrix products, per_device(): jnp.dot(normed_all, gate_full, preferred_element_type=jnp.float32)  9.71 us
  transfers between devices with their start and end apart: 8, of which 6 were waited for; matrix products, arithmetic and copies ran while one was open for 6% of the time, Pallas kernels for 0%

profile of v1, /device:TPU:0, one launch (start us, length us, event | category | flops | bytes accessed | tf_op | source)
XLA Modules:
  0.0 391.3 jit_solution(8543122711273827270)
XLA Ops:
  7.4 0.0 copy-start
  7.4 0.0 copy-start.5
  7.4 0.0 reduce-scatter.3.cloned.1.call-start
  7.4 1.0 fusion.19
  8.4 1.0 fusion.21
  9.4 4.9 %collective-permute-start.1 = (bf16[128,64]{0,1:T(8,128)(2,1)S(1)}, bf16[128,64]{0,1:T(8,128)(2,1)S(1)}, u32[]{:S(2)}, u32[]{:S(2)}) collective-permute-start(bf16[128,64]{0,1:T(8,128)(2,1)S(1)} %slice.18), channel_id=1, source_target_pairs={{0,4},{4,8},{8,12},{12,16},{16,20},{20,24},{24,28},{1,5},{5,9},{9,... | collective-permute-start | bytes 49160 | tf_op jit(solution)/shard_map/ppermute | solution.py:18
  14.3 0.7 slice.14
  15.0 3.4 collective-permute-start
  18.5 1.2 copy.19
  19.6 0.4 reshape.190
  20.1 0.1 bitcast_reduce_fusion
  20.3 0.8 multiply_convert_fusion.1
  21.1 0.0 copy-start.6
  21.1 0.1 or_or_fusion
  21.2 0.3 broadcast_and_fusion
  21.5 0.1 reshape_reshape.3
  21.6 0.0 copy-done.5
  21.6 0.1 reshape.186
  21.8 0.0 collective-permute-done.1
  21.9 0.1 reshape.188
  22.0 0.6 fusion.1
  22.7 0.0 copy-start.3
  22.7 0.0 copy-done.6
  22.7 0.1 broadcast_maximum_fusion
  22.8 1.6 copy-done.3
  24.3 0.7 fusion
  25.0 0.1 exponential_add_fusion
  25.1 0.0 collective-permute-done
  25.2 0.1 reshape.185
  25.3 2.8 fusion.12
  28.1 0.3 copy.22
  28.4 0.0 copy-done
  28.4 2.7 convolution_convert_fusion
  31.1 0.0 copy-start.1
  31.1 0.0 copy-start.7
  31.1 0.0 reduce-scatter.3.cloned.1.call-update
  31.1 0.0 copy-start.4
  31.1 0.0 all-gather.6.cloned.1.call-start
  31.2 0.5 all-gather.6.cloned.1.call-update
  31.7 0.0 all-gather.4.cloned.1.call-start
  31.8 37.5 %reduce-scatter.3.cloned.1.call-done = bf16[768,512]{1,0:T(8,128)(2,1)} async-done(((bf16[768,2048]{1,0:T(8,128)(2,1)}), bf16[768,512]{1,0:T(8,128)(2,1)}) %reduce-scatter.3.cloned.1.call-update) | async-done | bytes 786448 | tf_op jit(solution)/shard_map/reduce_scatter | solution.py:101
  69.2 0.0 copy-done.1
  69.2 1.5 fusion.2
  70.7 5.8 %psum.7 = f32[768]{0:T(1024)S(1)} all-reduce(f32[768]{0:T(1024)S(1)} %fusion.2), channel_id=1, replica_groups=mesh['sp'=8,'tp'=4] {'tp'}, use_global_device_ids=true, to_apply=%region_6.7 | all-reduce | flops 768 | bytes 6144 | tf_op jit(solution)/shard_map/psum | solution.py:105
  76.5 0.0 copy-done.7
  76.5 2.3 fusion.4
  78.8 0.0 all-gather.4.cloned.1.call-update
  78.8 0.0 copy-done.4
  78.8 2.9 stack.2
  81.7 5.7 %all-to-all-start = ((bf16[8,256,1408]{2,1,0:T(8,128)(2,1)}), bf16[8,256,1408]{2,1,0:T(8,128)(2,1)}, u32[]{:S(2)}, u32[]{:S(2)}) async-start(bf16[8,256,1408]{2,1,0:T(8,128)(2,1)} %stack.2), calls=%async_computation.1 | async-start | bytes 11534336 | tf_op jit(solution)/shard_map/all_to_all | solution.py:12
  87.5 0.0 all-gather.8.cloned.1.call-start
  87.5 0.5 all-gather.8.cloned.1.call-update
  88.0 0.2 reduce-scatter.5.cloned.1.call-start
  88.3 83.8 %all-gather.6.cloned.1.call-done = bf16[2048,1408]{1,0:T(8,128)(2,1)} async-done(((bf16[256,1408]{1,0:T(8,128)(2,1)}), bf16[2048,1408]{1,0:T(8,128)(2,1)}) %all-gather.6.cloned.1.call-update) | async-done | bytes 5767184 | tf_op jit(solution)/shard_map/all_gather | solution.py:51
  172.1 54.1 %all-gather.4.cloned.1.call-done = bf16[768,2048]{1,0:T(8,128)(2,1)} async-done(((bf16[768,512]{1,0:T(8,128)(2,1)}), bf16[768,2048]{1,0:T(8,128)(2,1)}) %all-gather.4.cloned.1.call-update) | async-done | bytes 3145744 | tf_op jit(solution)/shard_map/all_gather | solution.py:109
  226.2 9.7 %fusion.34 = f32[768,1408]{1,0:T(8,128)} fusion(bf16[768,2048]{1,0:T(8,128)(2,1)} %all-gather.4.cloned.1.call-done, bf16[2048,1408]{1,0:T(8,128)(2,1)} %all-gather.6.cloned.1.call-done), kind=kOutput, calls=%fused_computation.60 | convolution fusion | flops 4429185024 | bytes 13238272 | tf_op jit(solution)/shard_map/dot_general | solution.py:110
  235.9 26.1 %all-to-all-done = bf16[8,256,1408]{2,1,0:T(8,128)(2,1)} async-done(((bf16[8,256,1408]{2,1,0:T(8,128)(2,1)}), bf16[8,256,1408]{2,1,0:T(8,128)(2,1)}, u32[]{:S(2)}, u32[]{:S(2)}) %all-to-all-start) | async-done | bytes 5767200 | tf_op jit(solution)/shard_map/all_to_all | solution.py:12
  262.0 66.4 %all-gather.8.cloned.1.call-done = bf16[1408,2048]{1,0:T(8,128)(2,1)} async-done(((bf16[1408,256]{1,0:T(8,128)(2,1)}), bf16[1408,2048]{1,0:T(8,128)(2,1)}) %all-gather.8.cloned.1.call-update) | async-done | bytes 5767184 | tf_op jit(solution)/shard_map/all_gather | solution.py:54
  328.4 16.9 %convolution_convert_fusion.1 = bf16[768,2048]{1,0:T(8,128)(2,1)} fusion(bf16[1408,2048]{1,0:T(8,128)(2,1)} %all-gather.8.cloned.1.call-done, f32[768,1408]{1,0:T(8,128)} %fusion.34, bf16[768,2048]{1,0:T(8,128)(2,1)} %all-gather.4.cloned.1.call-done, bf16[2048,1408]{1,0:T(8,128)(2,1)} %bitcast.12), kind=kOutput, calls=%fused_computation.2 | convolution fusion | flops 8866430976 | bytes 22151168 | tf_op jit(solution)/shard_map/dot_general | solution.py:113
  345.3 0.0 copy-start.2
  345.3 0.0 reduce-scatter.5.cloned.1.call-update
  345.3 36.1 %reduce-scatter.5.cloned.1.call-done = bf16[768,512]{1,0:T(8,128)(2,1)} async-done(((bf16[768,2048]{1,0:T(8,128)(2,1)}), bf16[768,512]{1,0:T(8,128)(2,1)}) %reduce-scatter.5.cloned.1.call-update) | async-done | bytes 786448 | tf_op jit(solution)/shard_map/reduce_scatter | solution.py:114
  381.4 0.0 copy-done.2
  381.4 2.3 fusion.5
  (15 shorter events, 0.2 us)
Async XLA Ops:
  7.4 21.1 %copy-start = (bf16[256,2048]{1,0:T(8,128)(2,1)S(1)}, bf16[256,2048]{1,0:T(8,128)(2,1)}, u32[]{:S(2)}) copy-start(bf16[256,2048]{1,0:T(8,128)(2,1)} %param.18) | copy-start | bytes 3145732
  7.4 14.3 %copy-start.5 = (bf16[768,64]{0,1:T(8,128)(2,1)S(1)}, bf16[768,64]{0,1:T(8,128)(2,1)}, u32[]{:S(2)}) copy-start(bf16[768,64]{0,1:T(8,128)(2,1)} %param.14) | copy-start | bytes 294916
  7.4 61.9 %reduce-scatter.3.cloned.1.call-start = ((), (), s32[]{:S(2)}) async-start(), calls=%async_computation.3 | async-start | bytes 3932160 | tf_op jit(solution)/shard_map/reduce_scatter | solution.py:101
  9.4 12.4 %collective-permute-start.1 = (bf16[128,64]{0,1:T(8,128)(2,1)S(1)}, bf16[128,64]{0,1:T(8,128)(2,1)S(1)}, u32[]{:S(2)}, u32[]{:S(2)}) collective-permute-start(bf16[128,64]{0,1:T(8,128)(2,1)S(1)} %slice.18), channel_id=1, source_target_pairs={{0,4},{4,8},{8,12},{12,16},{16,20},{20,24},{24,28},{1,5},{5,9},{9,... | collective-permute-start | bytes 49160 | tf_op jit(solution)/shard_map/ppermute | solution.py:18
  15.0 10.1 %collective-permute-start = (bf16[128,64]{0,1:T(8,128)(2,1)S(1)}, bf16[128,64]{0,1:T(8,128)(2,1)S(1)}, u32[]{:S(2)}, u32[]{:S(2)}) collective-permute-start(bf16[128,64]{0,1:T(8,128)(2,1)S(1)} %slice.14), channel_id=1, source_target_pairs={{0,4},{4,8},{8,12},{12,16},{16,20},{20,24},{24,28},{1,5},{5,9},{9,... | collective-permute-start | bytes 49160 | tf_op jit(solution)/shard_map/ppermute | solution.py:18
  21.1 1.6 copy-start.6
  22.7 1.6 copy-start.3
  31.1 38.1 %copy-start.1 = (bf16[768,512]{1,0:T(8,128)(2,1)S(1)}, bf16[768,512]{1,0:T(8,128)(2,1)}, u32[]{:S(2)}) copy-start(bf16[768,512]{1,0:T(8,128)(2,1)} %param.19) | copy-start | bytes 2359300
  31.1 45.4 %copy-start.7 = (f32[512]{0:T(512)S(1)}, f32[512]{0:T(512)}, u32[]{:S(2)}) copy-start(f32[512]{0:T(512)} %param.20) | copy-start | bytes 6148
  31.1 47.7 %copy-start.4 = (bf16[256,1408]{1,0:T(8,128)(2,1)S(1)}, bf16[256,1408]{1,0:T(8,128)(2,1)}, u32[]{:S(2)}) copy-start(bf16[256,1408]{1,0:T(8,128)(2,1)} %param.22) | copy-start | bytes 2162692
  31.1 141.0 %all-gather.6.cloned.1.call-start = ((), (), s32[]{:S(2)}) async-start(), calls=%async_computation.5 | async-start | bytes 6488064 | tf_op jit(solution)/shard_map/all_gather | solution.py:51
  31.7 194.5 %all-gather.4.cloned.1.call-start = ((), (), s32[]{:S(2)}) async-start(), calls=%async_computation.4 | async-start | bytes 3932160 | tf_op jit(solution)/shard_map/all_gather | solution.py:109
  81.7 180.3 %all-to-all-start = ((bf16[8,256,1408]{2,1,0:T(8,128)(2,1)}), bf16[8,256,1408]{2,1,0:T(8,128)(2,1)}, u32[]{:S(2)}, u32[]{:S(2)}) async-start(bf16[8,256,1408]{2,1,0:T(8,128)(2,1)} %stack.2), calls=%async_computation.1 | async-start | bytes 11534336 | tf_op jit(solution)/shard_map/all_to_all | solution.py:12
  87.5 241.0 %all-gather.8.cloned.1.call-start = ((), (), s32[]{:S(2)}) async-start(), calls=%async_computation.6 | async-start | bytes 6488064 | tf_op jit(solution)/shard_map/all_gather | solution.py:54
  88.0 293.4 %reduce-scatter.5.cloned.1.call-start = ((), (), s32[]{:S(2)}) async-start(), calls=%async_computation.7 | async-start | bytes 3932160 | tf_op jit(solution)/shard_map/reduce_scatter | solution.py:114
  345.3 36.1 %copy-start.2 = (bf16[768,512]{1,0:T(8,128)(2,1)S(1)}, bf16[768,512]{1,0:T(8,128)(2,1)}, u32[]{:S(2)}) copy-start(bf16[768,512]{1,0:T(8,128)(2,1)} %reduce-scatter.3.cloned.1.call-done) | copy-start | bytes 2359300
Sparse Core Ops, SparseCore 0:
  31.3 37.9 reduce-scatter.2
  345.5 35.8 reduce-scatter.4
Sparse Core Ops, SparseCore 1:
  33.8 138.2 all-gather.5
  173.5 52.6 all-gather.3
  228.1 100.2 all-gather.7
